TPU v7x, 256 devices: a whole 4x4x8 slice. The times are simulated.
256 devices in a mesh: sp: 32 (over z, y), dp: 8 (over x, core).
Axes of the slice: x: 4, y: 4, z: 8, core: 2. Of those that a mesh axis runs over, the one named last changes fastest.
Arguments:
- queries: bfloat16 [8, 2048, 5120], P('dp', None, 'sp'), may hold values from -6 to 6
- keys: bfloat16 [8, 1024, 5120], P('dp', None, 'sp'), may hold values from -6 to 6
- values: bfloat16 [8, 1024, 5120], P('dp', None, 'sp'), may hold values from -48 to 48
- q_gain: float32 [64], replicated, may hold values from 0.5 to 10
- k_gain: float32 [64], replicated, may hold values from 0.5 to 10
- w_out: bfloat16 [2048, 2048], P(None, 'dp'), may hold values from -0.125 to 0.125
Outputs:
- mixed: bfloat16 [8, 5120, 2048], P('dp', 'sp')
All inputs are finite; a program needn't handle non-finite values.
Results may differ from a plain program's by a relative error of at most 0.0038.
The roundings to bfloat16 on the way count: a program that leaves them out, or rounds other values in their place, can miss the bound.
Values may be sent and summed in bfloat16 or wider, within the bound.
A program may use at most 64 MiB of HBM per device.

v0:
```python
import jax
import jax.numpy as jnp
from jax import lax
from jax.sharding import Mesh
from jax.sharding import PartitionSpec as P

HD = 64
QH = 32
KV = 16
GRID_W = 64
SP = ("sp_0", "sp_1")


epsilon = 1e-06
rotary_base = 10000.0
block_count = 8


def cut_along(value, dim, devices):
    before, after = (value.shape[:dim], value.shape[dim + 1 :])
    return jnp.moveaxis(value.reshape(*before, devices, -1, *after), dim, 0)


def joined_along(parts, dim):
    parts = jnp.moveaxis(parts, 0, dim)
    shape = parts.shape
    return parts.reshape(*shape[:dim], shape[dim] * shape[dim + 1], *shape[dim + 2 :])


def turned_blocks(parts, axes, turns):
    shape = [lax.axis_size(a) for a in axes]
    parts = parts.reshape(*shape, *parts.shape[1:])
    for k in turns:
        parts = lax.all_to_all(parts, axes[k], split_axis=k, concat_axis=k, tiled=True)
    return parts.reshape(-1, *parts.shape[len(axes) :])


def stepwise_exchange(value, axes, turns, split_dim, concat_dim):
    parts = cut_along(value, split_dim, lax.axis_size(axes))
    return joined_along(turned_blocks(parts, axes, turns), concat_dim)


def sent_together(arrays, axis, split_dim, concat_dim, along):
    widths = [a.shape[along] for a in arrays]
    both = jnp.concatenate(arrays, axis=along)
    out = lax.all_to_all(both, axis, split_axis=split_dim, concat_axis=concat_dim, tiled=True)
    return tuple(jnp.split(out, [sum(widths[:k]) for k in range(1, len(widths))], axis=along))


def swapped(block, axis, apart):
    count = lax.axis_size(axis)
    route = []
    for low in range(count):
        high = low | 1 << apart
        if high != low and high < count:
            route += [(low, high), (high, low)]
    return lax.ppermute(block, axis, route)


def rotary_tables(first_row, row_count):
    position = first_row + lax.iota(jnp.int32, row_count)
    grid_row = (position // GRID_W).astype(jnp.float32)
    grid_col = (position % GRID_W).astype(jnp.float32)
    quarter = HD // 4
    inv_freq = rotary_base ** (-(2.0 * lax.iota(jnp.float32, quarter)) / (HD // 2))
    row_angle = inv_freq[:, None] * grid_row[None, :]
    col_angle = inv_freq[:, None] * grid_col[None, :]
    cos_table = jnp.concatenate(
        [jnp.cos(row_angle), jnp.cos(row_angle), jnp.cos(col_angle), jnp.cos(col_angle)], axis=0
    )
    sin_table = jnp.concatenate(
        [jnp.sin(row_angle), jnp.sin(row_angle), jnp.sin(col_angle), jnp.sin(col_angle)], axis=0
    )
    return (cos_table, sin_table)


def normalize_turn(field, gain, cos_table, sin_table):
    head_count = field.shape[0] // HD
    values_f = field.astype(jnp.float32).reshape(head_count, HD, field.shape[1])
    normed = (
        values_f
        * lax.rsqrt(jnp.mean(values_f * values_f, axis=1, keepdims=True) + epsilon)
        * gain[None, :, None]
    )
    quarter = HD // 4
    quarters_of = normed.reshape(head_count, 4, quarter, field.shape[1])
    turned = jnp.concatenate(
        [-quarters_of[:, 1], quarters_of[:, 0], -quarters_of[:, 3], quarters_of[:, 2]], axis=1
    )
    return (normed * cos_table[None] + turned * sin_table[None]).astype(jnp.bfloat16)


def attention_heads(query_heads, key_heads, value_heads, seq_len):
    kv_local = key_heads.shape[0]
    group_local = query_heads.shape[0] // kv_local
    query_split = query_heads.reshape(kv_local, group_local, HD, seq_len)
    score_scale = HD ** (-0.5)
    block_rows = seq_len // block_count

    def one_block(block_index, result):
        row_start = block_index * block_rows
        query_block = lax.dynamic_slice_in_dim(query_split, row_start, block_rows, 3)
        scores = (
            jnp.einsum("hgdq,hdk->hgqk", query_block, key_heads, preferred_element_type=jnp.float32)
            * score_scale
        )
        row_max = jnp.max(scores, axis=-1, keepdims=True)
        weights = jnp.exp(scores - row_max)
        weights = (weights / jnp.sum(weights, axis=-1, keepdims=True)).astype(jnp.bfloat16)
        attended = jnp.einsum(
            "hgqk,hdk->hgdq", weights, value_heads, preferred_element_type=jnp.float32
        )
        return lax.dynamic_update_slice_in_dim(result, attended.astype(jnp.bfloat16), row_start, 3)

    result = jnp.zeros(query_split.shape, jnp.bfloat16)
    result = lax.fori_loop(0, block_count, one_block, result)
    return result.reshape(query_heads.shape)


def on_device(queries, keys, values, q_gain, k_gain, w_out):
    sp_count = lax.axis_size(SP)
    tok_rows = queries.shape[2]
    seq_len = tok_rows * sp_count
    cos_table, sin_table = rotary_tables(lax.axis_index(SP) * tok_rows, tok_rows)
    query_rot = normalize_turn(queries[0], q_gain, cos_table, sin_table)
    key_rot = normalize_turn(keys[0], k_gain, cos_table, sin_table)
    value_rows = values[0].reshape(KV, HD, tok_rows)
    query_heads = stepwise_exchange(query_rot, SP, (0, 1), 0, 2)
    share_count = max(sp_count // KV, 1)
    part_rows = tok_rows // share_count
    key_cut = (
        key_rot.reshape(KV, HD, share_count, part_rows)
        .transpose(0, 2, 1, 3)
        .reshape(KV * share_count, HD, part_rows)
    )
    value_cut = (
        value_rows.reshape(KV, HD, share_count, part_rows)
        .transpose(0, 2, 1, 3)
        .reshape(KV * share_count, HD, part_rows)
    )
    key_got, value_got = sent_together((key_cut, value_cut), SP, 0, 2, 1)
    kv_local = key_got.shape[0]
    key_got = key_got.reshape(kv_local, HD, sp_count, part_rows)
    value_got = value_got.reshape(kv_local, HD, sp_count, part_rows)
    key_other, value_other = swapped((key_got, value_got), SP, 0)
    key_got = jnp.concatenate([key_got, key_other], axis=3)
    value_got = jnp.concatenate([value_got, value_other], axis=3)
    key_heads = key_got.reshape(kv_local, HD, seq_len)
    value_heads = value_got.reshape(kv_local, HD, seq_len)
    attended = attention_heads(query_heads, key_heads, value_heads, seq_len)
    token_heads = stepwise_exchange(attended, SP, (0, 1), 2, 0)
    token_rows = token_heads.reshape(QH * HD, tok_rows)
    product = lax.dot_general(
        token_rows,
        lax.all_gather(w_out, "dp", axis=1, tiled=True),
        (((0,), (0,)), ((), ())),
        preferred_element_type=jnp.float32,
    )
    mixed_rows = product.astype(jnp.bfloat16)
    return mixed_rows[None]


def solution(mesh):
    torus = Mesh(mesh.devices.reshape(8, 4, mesh.shape["dp"]), ("sp_0", "sp_1", "dp"))
    return jax.shard_map(
        on_device,
        mesh=torus,
        in_specs=(P("dp", None, SP), P("dp", None, SP), P("dp", None, SP), P(), P(), P(None, "dp")),
        out_specs=P("dp", SP, None),
        check_vma=False,
    )
```

profile of v0, /device:TPU:2, one launch (start us, length us, event | category | flops | bytes accessed | tf_op | source)
XLA Modules:
  0.0 241.0 jit_solution(1003949146622194694)
XLA Ops:
  6.5 1.3 reshape.250
  7.9 1.2 copy.100
  9.5 0.4 multiply_reduce_fusion.1
  10.0 3.6 %copy.101 = f32[16,4,16,160]{2,0,3,1:T(8,128)} copy(f32[16,4,16,160]{3,2,1,0:T(8,128)S(1)} %bitcast.85) | data formatting | bytes 1310720 | tf_op jit(solution)/shard_map/convert_element_type | solution.py:79
  13.7 3.1 %multiply_multiply_fusion = f32[16,4,16,160]{2,0,3,1:T(8,128)S(1)} fusion(f32[16,4,16,160]{2,0,3,1:T(8,128)} %copy.101, f32[4,16]{1,0:T(4,128)S(1)} %mul.221, f32[16,160]{0,1:T(8,128)S(1)} %add_rsqrt_fusion), kind=kLoop, calls=%fused_computation.15 | loop fusion | flops 327680 | bytes 1321216 | tf_op jit(solution)/shard_map/mul | solution.py:81
  17.1 1.6 fusion.18
  19.7 0.4 reshape_reshape_squeeze.3
  20.1 0.6 copy.103
  20.7 0.9 copy.104
  22.0 1.1 copy.105
  23.1 11.6 %all-to-all-start.2 = ((bf16[32,128,80]{1,2,0:T(8,128)(2,1)}), bf16[32,128,80]{1,2,0:T(8,128)(2,1)}, u32[]{:S(2)}, u32[]{:S(2)}) async-start(bf16[32,128,80]{1,2,0:T(8,128)(2,1)} %copy.105), calls=%async_computation.2 | async-start | bytes 1310720 | tf_op jit(solution)/shard_map/all_to_all | solution.py:46
  34.7 0.5 copy.92
  35.2 1.5 convert_multiply_fusion
  36.9 0.5 copy-done.3
  37.5 1.8 reduce_sum.29
  39.3 0.4 multiply_multiply_fusion.1
  40.1 1.6 fusion.19
  41.7 13.3 %all-to-all-done.2 = bf16[32,128,80]{1,2,0:T(8,128)(2,1)} async-done(((bf16[32,128,80]{1,2,0:T(8,128)(2,1)}), bf16[32,128,80]{1,2,0:T(8,128)(2,1)}, u32[]{:S(2)}, u32[]{:S(2)}) %all-to-all-start.2) | async-done | bytes 655392 | tf_op jit(solution)/shard_map/all_to_all | solution.py:46
  54.9 3.6 %all-to-all-start = ((bf16[8,4,1,64,160]{4,3,1,2,0:T(8,128)(2,1)}), bf16[8,4,1,64,160]{4,3,1,2,0:T(8,128)(2,1)S(1)}, u32[]{:S(2)}, u32[]{:S(2)}) async-start(bf16[8,4,1,64,160]{4,3,1,2,0:T(8,128)(2,1)} %fusion.19), calls=%async_computation | async-start | bytes 2097152 | tf_op jit(solution)/shard_map/all_to_all | solution.py:34
  58.5 1.5 fusion.23
  60.0 0.8 copy.109
  60.8 1.3 collective-permute-start.1
  62.1 23.7 %all-to-all-done = bf16[8,4,1,64,160]{4,3,1,2,0:T(8,128)(2,1)S(1)} async-done(((bf16[8,4,1,64,160]{4,3,1,2,0:T(8,128)(2,1)}), bf16[8,4,1,64,160]{4,3,1,2,0:T(8,128)(2,1)S(1)}, u32[]{:S(2)}, u32[]{:S(2)}) %all-to-all-start) | async-done | bytes 655392 | tf_op jit(solution)/shard_map/all_to_all | solution.py:34
  85.8 1.1 copy.96
  86.9 3.9 %all-to-all-start.1 = ((bf16[8,4,1,64,160]{4,3,0,2,1:T(8,128)(2,1)}), bf16[8,4,1,64,160]{4,3,0,2,1:T(8,128)(2,1)S(1)}, u32[]{:S(2)}, u32[]{:S(2)}) async-start(bf16[8,4,1,64,160]{4,3,0,2,1:T(8,128)(2,1)} %copy.96), calls=%async_computation.1 | async-start | bytes 2097152 | tf_op jit(solution)/shard_map/all_to_all | solution.py:34
  90.8 1.5 copy.107
  92.3 2.0 collective-permute-start
  94.4 1.6 pad_maximum_fusion.1
  95.9 2.5 %reshape.246 = bf16[1,64,5120]{2,1,0:T(8,128)(2,1)} reshape(bf16[1,64,32,160]{3,2,1,0:T(8,128)(2,1)S(1)} %pad_maximum_fusion.1) | data formatting | bytes 1310720 | tf_op jit(solution)/shard_map/reshape | solution.py:149
  98.4 17.3 %collective-permute-done = bf16[1,64,32,80]{3,2,1,0:T(8,128)(2,1)} collective-permute-done((bf16[1,64,32,80]{3,2,1,0:T(8,128)(2,1)}, bf16[1,64,32,80]{3,2,1,0:T(8,128)(2,1)}, u32[]{:S(2)}, u32[]{:S(2)}) %collective-permute-start) | collective-permute-done | bytes 327712 | tf_op jit(solution)/shard_map/ppermute | solution.py:57
  115.8 1.7 pad_maximum_fusion
  117.5 1.7 reshape.244
  119.3 0.6 copy.98
  119.9 1.7 reshape_reshape.7
  121.7 57.9 %while.13 = (s32[]{:T(128)}, bf16[1,1,64,5120]{3,2,1,0:T(8,128)(2,1)S(1)}, bf16[1,1,64,5120]{3,2,1,0:T(8,128)(2,1)S(1)}, bf16[1,64,5120]{2,1,0:T(8,128)(2,1)S(1)...) while((s32[]{:T(128)}, bf16[1,1,64,5120]{3,2,1,0:T(8,128)(2,1)S(1)}, ...), condition=%wide.region_5.6_spmd, body=%wide.region_2.5_spmd.sunk | while | flops 868391680 | bytes 40812176 | solution.py:116
  121.9 2.0 multiply_reduce_fusion.3
  123.9 2.3 fusion.31
  126.2 2.9 %fusion.32 = bf16[1,1,64,5120]{3,2,1,0:T(8,128)(2,1)S(1)} fusion(bf16[1,1,64,5120]{3,2,1,0:T(8,128)(2,1)S(1)} %get-tuple-element.177, s32[]{:T(128)S(6)} %select_n.37, f32[640,5120]{1,0:T(8,128)S(1)} %get-tuple-element.165, f32[640]{0:T(1024)S(1)} %fusion.31, f32[640]{0:T(1024)S(1)} %get-tuple-element.166, ...), kind=kOutput, calls=%fused_computation.7.clone.1 | convolution fusion | flops 432578560 | bytes 13852676 | tf_op jit(solution)/shard_map/while/body/eval_jaxpr/hgqk,hdk->hgdq/dot_general | solution.py:110
  129.2 2.0 multiply_reduce_fusion.3
  131.1 2.3 fusion.31
  133.4 2.9 %fusion.32 = bf16[1,1,64,5120]{3,2,1,0:T(8,128)(2,1)S(1)} fusion(bf16[1,1,64,5120]{3,2,1,0:T(8,128)(2,1)S(1)} %get-tuple-element.177, s32[]{:T(128)S(6)} %select_n.37, f32[640,5120]{1,0:T(8,128)S(1)} %get-tuple-element.165, f32[640]{0:T(1024)S(1)} %fusion.31, f32[640]{0:T(1024)S(1)} %get-tuple-element.166, ...), kind=kOutput, calls=%fused_computation.7.clone.1 | convolution fusion | flops 432578560 | bytes 13852676 | tf_op jit(solution)/shard_map/while/body/eval_jaxpr/hgqk,hdk->hgdq/dot_general | solution.py:110
  136.4 2.0 multiply_reduce_fusion.3
  138.3 2.3 fusion.31
  140.6 3.0 %fusion.32 = bf16[1,1,64,5120]{3,2,1,0:T(8,128)(2,1)S(1)} fusion(bf16[1,1,64,5120]{3,2,1,0:T(8,128)(2,1)S(1)} %get-tuple-element.177, s32[]{:T(128)S(6)} %select_n.37, f32[640,5120]{1,0:T(8,128)S(1)} %get-tuple-element.165, f32[640]{0:T(1024)S(1)} %fusion.31, f32[640]{0:T(1024)S(1)} %get-tuple-element.166, ...), kind=kOutput, calls=%fused_computation.7.clone.1 | convolution fusion | flops 432578560 | bytes 13852676 | tf_op jit(solution)/shard_map/while/body/eval_jaxpr/hgqk,hdk->hgdq/dot_general | solution.py:110
  143.6 2.0 multiply_reduce_fusion.3
  145.6 2.3 fusion.31
  147.8 2.9 %fusion.32 = bf16[1,1,64,5120]{3,2,1,0:T(8,128)(2,1)S(1)} fusion(bf16[1,1,64,5120]{3,2,1,0:T(8,128)(2,1)S(1)} %get-tuple-element.177, s32[]{:T(128)S(6)} %select_n.37, f32[640,5120]{1,0:T(8,128)S(1)} %get-tuple-element.165, f32[640]{0:T(1024)S(1)} %fusion.31, f32[640]{0:T(1024)S(1)} %get-tuple-element.166, ...), kind=kOutput, calls=%fused_computation.7.clone.1 | convolution fusion | flops 432578560 | bytes 13852676 | tf_op jit(solution)/shard_map/while/body/eval_jaxpr/hgqk,hdk->hgdq/dot_general | solution.py:110
  150.8 2.0 multiply_reduce_fusion.3
  152.8 2.3 fusion.31
  155.0 2.9 %fusion.32 = bf16[1,1,64,5120]{3,2,1,0:T(8,128)(2,1)S(1)} fusion(bf16[1,1,64,5120]{3,2,1,0:T(8,128)(2,1)S(1)} %get-tuple-element.177, s32[]{:T(128)S(6)} %select_n.37, f32[640,5120]{1,0:T(8,128)S(1)} %get-tuple-element.165, f32[640]{0:T(1024)S(1)} %fusion.31, f32[640]{0:T(1024)S(1)} %get-tuple-element.166, ...), kind=kOutput, calls=%fused_computation.7.clone.1 | convolution fusion | flops 432578560 | bytes 13852676 | tf_op jit(solution)/shard_map/while/body/eval_jaxpr/hgqk,hdk->hgdq/dot_general | solution.py:110
  158.0 2.0 multiply_reduce_fusion.3
  160.0 2.3 fusion.31
  162.2 2.9 %fusion.32 = bf16[1,1,64,5120]{3,2,1,0:T(8,128)(2,1)S(1)} fusion(bf16[1,1,64,5120]{3,2,1,0:T(8,128)(2,1)S(1)} %get-tuple-element.177, s32[]{:T(128)S(6)} %select_n.37, f32[640,5120]{1,0:T(8,128)S(1)} %get-tuple-element.165, f32[640]{0:T(1024)S(1)} %fusion.31, f32[640]{0:T(1024)S(1)} %get-tuple-element.166, ...), kind=kOutput, calls=%fused_computation.7.clone.1 | convolution fusion | flops 432578560 | bytes 13852676 | tf_op jit(solution)/shard_map/while/body/eval_jaxpr/hgqk,hdk->hgdq/dot_general | solution.py:110
  165.2 2.0 multiply_reduce_fusion.3
  167.2 2.3 fusion.31
  169.5 2.9 %fusion.32 = bf16[1,1,64,5120]{3,2,1,0:T(8,128)(2,1)S(1)} fusion(bf16[1,1,64,5120]{3,2,1,0:T(8,128)(2,1)S(1)} %get-tuple-element.177, s32[]{:T(128)S(6)} %select_n.37, f32[640,5120]{1,0:T(8,128)S(1)} %get-tuple-element.165, f32[640]{0:T(1024)S(1)} %fusion.31, f32[640]{0:T(1024)S(1)} %get-tuple-element.166, ...), kind=kOutput, calls=%fused_computation.7.clone.1 | convolution fusion | flops 432578560 | bytes 13852676 | tf_op jit(solution)/shard_map/while/body/eval_jaxpr/hgqk,hdk->hgdq/dot_general | solution.py:110
  172.4 2.0 multiply_reduce_fusion.3
  174.4 2.3 fusion.31
  176.7 2.9 %fusion.32 = bf16[1,1,64,5120]{3,2,1,0:T(8,128)(2,1)S(1)} fusion(bf16[1,1,64,5120]{3,2,1,0:T(8,128)(2,1)S(1)} %get-tuple-element.177, s32[]{:T(128)S(6)} %select_n.37, f32[640,5120]{1,0:T(8,128)S(1)} %get-tuple-element.165, f32[640]{0:T(1024)S(1)} %fusion.31, f32[640]{0:T(1024)S(1)} %get-tuple-element.166, ...), kind=kOutput, calls=%fused_computation.7.clone.1 | convolution fusion | flops 432578560 | bytes 13852676 | tf_op jit(solution)/shard_map/while/body/eval_jaxpr/hgqk,hdk->hgdq/dot_general | solution.py:110
  179.6 1.3 reshape_reshape.8
  181.0 0.6 copy.110
  181.5 30.4 %all_to_all.38 = bf16[8,4,1,64,160]{4,3,1,2,0:T(8,128)(2,1)S(1)} all-to-all(bf16[8,4,1,64,160]{4,3,1,2,0:T(8,128)(2,1)S(1)} %bitcast.84), channel_id=1, replica_groups=mesh['sp_0'=8,'sp_1'=4,'dp'=8] {'sp_0'}, dimensions={0} | all-to-all | bytes 1310720 | tf_op jit(solution)/shard_map/all_to_all | solution.py:34
  212.0 16.2 %all_to_all.39 = bf16[8,4,1,64,160]{4,3,0,2,1:T(8,128)(2,1)S(1)} all-to-all(bf16[8,4,1,64,160]{4,3,0,2,1:T(8,128)(2,1)S(1)} %copy.111), channel_id=1, replica_groups=mesh['sp_0'=8,'sp_1'=4,'dp'=8] {'sp_1'}, dimensions={1} | all-to-all | bytes 1310720 | tf_op jit(solution)/shard_map/all_to_all | solution.py:34
  228.4 5.8 %fusion.12 = bf16[1,160,2048]{2,1,0:T(8,128)(2,1)} fusion(bf16[2048,160]{1,0:T(8,128)(2,1)S(1)} %bitcast.82, bf16[2048,2048]{1,0:T(8,128)(2,1)} %all-gather.2.cloned.1.call-done), kind=kOutput, calls=%fused_computation.17 | convolution fusion | flops 1342504960 | bytes 9699328 | tf_op jit(solution)/shard_map/dot_general | solution.py:153
  (37 shorter events, 3.1 us)
Async XLA Ops:
  10.0 3.6 %copy-start.4 = (f32[64]{0:T(128)S(1)}, f32[64]{0:T(128)}, u32[]{:S(2)}) copy-start(f32[64]{0:T(128)} %param.12) | copy-start | bytes 772
  18.7 1.0 copy-start.2
  21.6 13.1 %copy-start = (bf16[1,2048,160]{1,2,0:T(8,128)(2,1)S(1)}, bf16[1,2048,160]{1,2,0:T(8,128)(2,1)}, u32[]{:S(2)}) copy-start(bf16[1,2048,160]{1,2,0:T(8,128)(2,1)} %param.8) | copy-start | bytes 1966084
  23.1 31.8 %all-to-all-start.2 = ((bf16[32,128,80]{1,2,0:T(8,128)(2,1)}), bf16[32,128,80]{1,2,0:T(8,128)(2,1)}, u32[]{:S(2)}, u32[]{:S(2)}) async-start(bf16[32,128,80]{1,2,0:T(8,128)(2,1)} %copy.105), calls=%async_computation.2 | async-start | bytes 1310720 | tf_op jit(solution)/shard_map/all_to_all | solution.py:46
  36.7 0.7 copy-start.3
  54.9 30.8 %all-to-all-start = ((bf16[8,4,1,64,160]{4,3,1,2,0:T(8,128)(2,1)}), bf16[8,4,1,64,160]{4,3,1,2,0:T(8,128)(2,1)S(1)}, u32[]{:S(2)}, u32[]{:S(2)}) async-start(bf16[8,4,1,64,160]{4,3,1,2,0:T(8,128)(2,1)} %fusion.19), calls=%async_computation | async-start | bytes 2097152 | tf_op jit(solution)/shard_map/all_to_all | solution.py:34
  60.8 33.5 %collective-permute-start.1 = (bf16[1,64,32,80]{3,2,1,0:T(8,128)(2,1)S(1)}, bf16[1,64,32,80]{3,2,1,0:T(8,128)(2,1)}, u32[]{:S(2)}, u32[]{:S(2)}) collective-permute-start(bf16[1,64,32,80]{3,2,1,0:T(8,128)(2,1)S(1)} %copy.109), channel_id=1, source_target_pairs={{0,8},{8,0},{16,24},{24,16},{32,40},{40,32},{48,56},{56,48},{64,72... | collective-permute-start | bytes 983048 | tf_op jit(solution)/shard_map/ppermute | solution.py:57
  86.9 32.3 %all-to-all-start.1 = ((bf16[8,4,1,64,160]{4,3,0,2,1:T(8,128)(2,1)}), bf16[8,4,1,64,160]{4,3,0,2,1:T(8,128)(2,1)S(1)}, u32[]{:S(2)}, u32[]{:S(2)}) async-start(bf16[8,4,1,64,160]{4,3,0,2,1:T(8,128)(2,1)} %copy.96), calls=%async_computation.1 | async-start | bytes 2097152 | tf_op jit(solution)/shard_map/all_to_all | solution.py:34
  90.8 137.6 %all-gather.2.cloned.1.call-start = ((), (), s32[]{:S(2)}) async-start(), calls=%async_computation.5 | async-start | bytes 9437184 | tf_op jit(solution)/shard_map/all_gather | solution.py:155
  92.3 23.5 %collective-permute-start = (bf16[1,64,32,80]{3,2,1,0:T(8,128)(2,1)}, bf16[1,64,32,80]{3,2,1,0:T(8,128)(2,1)}, u32[]{:S(2)}, u32[]{:S(2)}) collective-permute-start(bf16[1,64,32,80]{3,2,1,0:T(8,128)(2,1)} %copy.107), channel_id=1, source_target_pairs={{0,8},{8,0},{16,24},{24,16},{32,40},{40,32},{48,56},{56,48},{64,72... | collective-permute-start | bytes 983048 | tf_op jit(solution)/shard_map/ppermute | solution.py:57
  119.3 2.4 copy-start.1
Sparse Core Ops, SparseCore 0:
  94.5 51.8 all-gather.1
where the time goes:
time: 242 us; the launch traced here: 241 us
  waiting for transfers between devices  54.3 us (22%)
  blocking collectives  46.6 us (19%)
  matrix products  45.2 us (19%)
  other arithmetic  33.4 us (14%)
  local copies, waits for them, and re-layouts  25 us (10%)
  starting transfers between devices  22.3 us (9%)
  between operations  13.8 us (6%)
    all_to_all x2, blocking collectives, turned_blocks(): lax.all_to_all(parts, axes[k], split_axis=k, concat_axis=k, tiled=True)  46.6 us
    all_to_all x2, waiting for transfers between devices, turned_blocks(): lax.all_to_all(parts, axes[k], split_axis=k, concat_axis=k, tiled=True)  23.7 us
    dot_general x8, matrix products, one_block(): jnp.einsum('hgqk,hdk->hgdq', weights, value_heads, preferred_element_type...  23.6 us
    reduce_sum x8, other arithmetic, one_block(): jnp.sum(weights, axis=-1, keepdims=True)  18.1 us
    ppermute x2, waiting for transfers between devices, swapped(): return lax.ppermute(block, axis, route)  17.3 us
    dot_general x8, matrix products, one_block(): jnp.einsum('hgdq,hdk->hgqk', query_block, key_heads, preferred_element_ty...  15.8 us
    all_to_all x1, waiting for transfers between devices, sent_together(): lax.all_to_all(both, axis, split_axis=split_dim, concat_axis=concat_dim,...  13.3 us
    all_to_all x1, starting transfers between devices, sent_together(): lax.all_to_all(both, axis, split_axis=split_dim, concat_axis=concat_dim,...  11.6 us
  transfers between devices with their start and end apart: 6, of which 3 were waited for; matrix products, arithmetic and copies ran while one was open for 34% of the time, Pallas kernels for 0%

commit v1 on v0

v1 whole, which is shorter than its diff:
```python
import jax
import jax.numpy as jnp
from jax import lax
from jax.experimental import pallas as pl
from jax.experimental.pallas import tpu as pltpu
from jax.sharding import PartitionSpec as P

HD = 64
QH = 32
KV = 16
GRID_W = 64
Z = 8
Y = 4
X = 4
TOK = 160
KEYS = 5120
TQ = 256
TILES = 20
KC = 256
GROUP = 4
SPAN = GROUP * TOK
W_ROWS = 2048
W_COLS = 256

epsilon = 1e-06
rotary_base = 10000.0
log2_scale = HD ** (-0.5) * 1.4426950408889634
f32 = jnp.float32
bf16 = jnp.bfloat16
MESH = pl.DeviceIdType.MESH


def rotary_tables(first_row, row_count):
    position = first_row + lax.iota(jnp.int32, row_count)
    grid_row = (position // GRID_W).astype(f32)
    grid_col = (position % GRID_W).astype(f32)
    quarter = HD // 4
    inv_freq = rotary_base ** (-(2.0 * lax.iota(f32, quarter)) / (HD // 2))
    row_angle = inv_freq[:, None] * grid_row[None, :]
    col_angle = inv_freq[:, None] * grid_col[None, :]
    cos_table = jnp.concatenate(
        [jnp.cos(row_angle), jnp.cos(row_angle), jnp.cos(col_angle), jnp.cos(col_angle)], axis=0
    )
    sin_table = jnp.concatenate(
        [jnp.sin(row_angle), jnp.sin(row_angle), jnp.sin(col_angle), jnp.sin(col_angle)], axis=0
    )
    return (cos_table, sin_table)


def turned(field, gain, cos_table, sin_table):
    u = field.astype(f32)
    n = u * lax.rsqrt(jnp.mean(u * u, axis=0, keepdims=True) + epsilon) * gain
    rot = jnp.concatenate([-n[16:32], n[0:16], -n[48:64], n[32:48]], axis=0)
    return n * cos_table + rot * sin_table


class Place:
    def __init__(self):
        sp = lax.axis_index("sp")
        self.dp = lax.axis_index("dp")
        self.z, self.y = lax.div(sp, Y), lax.rem(sp, Y)
        self.g = lax.div(self.y, 2)
        self.e = self.g * (3 - self.y) + (1 - self.g) * self.y
        self.head = 2 * self.z + self.e
        self.partner = self.z * Y + 3 - self.y
        x, self.c = lax.div(self.dp, 2), lax.rem(self.dp, 2)
        self.left = lax.rem(x + X - 1, X) * 2 + self.c
        self.right = lax.rem(x + 1, X) * 2 + self.c
        self.sib = self.dp + 1 - 2 * self.c
        self.opp = lax.rem(x + 2, X) * 2 + self.c

    def offset(self, n):
        i = lax.div(n, 2)
        return lax.div(i + 1, 2) * (2 * lax.rem(i, 2) - 1)

    def at(self, z, e):
        return z * Y + self.g * 3 + e * (1 - 2 * self.g)

    def target_z(self, n):
        return lax.rem(self.z + self.offset(n) + Z, Z)

    def source_z(self, n):
        return lax.rem(self.z - self.offset(n) + Z, Z)

    def slot_there(self, n):
        return 2 * lax.div(n, 2) + self.e


def loop(count, body):
    def step(n, carry):
        body(n)
        return carry

    lax.fori_loop(0, count, step, 0)


def attention_step(q, top, scale, kk, vt, x_ref, y_ref, scores=True, exps=True, sums=True):
    m = jnp.full((8, TQ), -jnp.inf, f32)
    total = jnp.zeros((8, TQ), f32)
    out = None
    for j in range(KEYS // KC):
        at = slice(j * KC, (j + 1) * KC)
        if sums:
            weights = (x_ref[at, :] * scale).astype(bf16)
            part = lax.dot_general(
                vt[:, at], weights, (((1,), (0,)), ((), ())), preferred_element_type=f32
            )
            out = part if out is None else out + part
        if scores:
            k = kk[at, :]
            s = lax.dot_general(
                jnp.concatenate([k, k], axis=1), q, (((1,), (0,)), ((), ())), preferred_element_type=f32
            )
            x_ref[at, :] = s
            m = jnp.maximum(m, jnp.max(s.reshape(KC // 8, 8, TQ), axis=0))
        if exps:
            e = jnp.exp2(y_ref[at, :] - top)
            y_ref[at, :] = e
            total = total + jnp.sum(e.reshape(KC // 8, 8, TQ), axis=0)
    return m, total, out


def layer(
    q_ref, k_ref, v_ref, w_ref, cos_ref, sin_ref, qg_ref, kg_ref, out_ref,
    kvs, qs, kvr, qr, kk, vt, qt, s0, s1, ot, atts, attr, wf,
    kv_ss, kv_rs, fw_ss, fw_rs, q_ss, q_rs, at_ss, at_rs, w_ss, w_rs, own_sem,
):
    me = Place()

    def remote(src, dst, ss, rs, **device):
        return pltpu.make_async_remote_copy(
            src_ref=src, dst_ref=dst, send_sem=ss, recv_sem=rs, device_id=device, device_id_type=MESH
        )

    barrier = pltpu.get_barrier_semaphore()

    def hello(**device):
        pl.semaphore_signal(barrier, inc=1, device_id=device, device_id_type=MESH)

    def greet(n):
        @pl.when(n != me.e)
        def _():
            hello(sp=me.at(me.target_z(n), lax.rem(n, 2)))

    loop(16, greet)
    hello(sp=me.partner)
    hello(dp=me.sib)
    hello(dp=me.left)
    hello(dp=me.right)

    cos_table, sin_table = cos_ref[...], sin_ref[...]

    def make_kv(n):
        j = 2 * me.target_z(n) + lax.rem(n, 2)
        rows = pl.ds(pl.multiple_of(j * HD, HD), HD)
        k = turned(k_ref[0, rows, :], kg_ref[...], cos_table, sin_table)
        both = jnp.concatenate([k, v_ref[0, rows, :].astype(f32)], axis=0)
        kvs[n] = jnp.transpose(both).astype(bf16)

    def make_q(n):
        j = 2 * me.target_z(n) + lax.rem(n, 2)
        a = q_ref[0, pl.ds(pl.multiple_of(j * 2 * HD, HD), HD), :]
        b = q_ref[0, pl.ds(pl.multiple_of(j * 2 * HD + HD, HD), HD), :]
        both = jnp.concatenate(
            [turned(a, qg_ref[...], cos_table, sin_table), turned(b, qg_ref[...], cos_table, sin_table)],
            axis=0,
        )
        qs[n] = jnp.transpose(both).astype(bf16)

    def kv_copy(n):
        there = me.slot_there(n)
        return remote(
            kvs.at[n], kvr.at[0, there], kv_ss.at[n], kv_rs.at[there],
            sp=me.at(me.target_z(n), lax.rem(n, 2)),
        )

    def q_copy(n):
        there = me.slot_there(n)
        return remote(
            qs.at[n], qr.at[there], q_ss.at[n], q_rs.at[there],
            sp=me.at(me.target_z(n), lax.rem(n, 2)),
        )

    def fw_copy(n):
        return remote(kvr.at[0, n], kvr.at[1, n], fw_ss.at[n], fw_rs.at[n], sp=me.partner)

    def at_copy(n):
        return remote(
            atts.at[n], attr.at[me.head], at_ss.at[n], at_rs.at[me.head],
            sp=me.at(me.source_z(n), lax.rem(n, 2)),
        )

    def arrival(ref, ss, rs):
        return remote(ref, ref, ss, rs, sp=me.partner)

    top_half, low_half = pl.ds(0, W_ROWS // 2), pl.ds(W_ROWS // 2, W_ROWS // 2)

    def w_copy(kind, src, dst, dp):
        return remote(src, dst, w_ss.at[kind], w_rs.at[kind], dp=dp)

    w_own = (
        w_copy(0, w_ref, wf.at[me.dp], me.sib),
        w_copy(1, w_ref, wf.at[me.dp], me.right),
        w_copy(2, w_ref, wf.at[me.dp], me.left),
    )
    w_next = (
        w_copy(3, wf.at[me.left, top_half], wf.at[me.left, top_half], me.right),
        w_copy(4, wf.at[me.right, low_half], wf.at[me.right, low_half], me.left),
        w_copy(5, wf.at[me.left], wf.at[me.left], me.sib),
        w_copy(6, wf.at[me.right], wf.at[me.right], me.sib),
    )
    w_last = (
        w_copy(7, wf.at[me.opp, top_half], wf.at[me.opp, top_half], me.sib),
        w_copy(8, wf.at[me.opp, low_half], wf.at[me.opp, low_half], me.sib),
    )

    def w_arrival(kind, ref):
        arrival(ref, w_ss.at[kind], w_rs.at[kind]).wait_recv()

    loop(16, make_kv)
    pl.semaphore_wait(barrier, 19)

    def send_kv(n):
        @pl.when(n != me.e)
        def _():
            kv_copy(n).start()

        make_q(n)

    loop(16, send_kv)

    def send_q(n):
        @pl.when(n != me.e)
        def _():
            q_copy(n).start()

    loop(16, send_q)
    own_w = pltpu.make_async_copy(w_ref, wf.at[me.dp], own_sem)
    own_w.start()
    for copy in w_own:
        copy.start()
    kvr[0, me.e] = kvs[me.e]
    qr[me.e] = qs[me.e]

    def forward(n):
        @pl.when(n != me.e)
        def _():
            arrival(kvr.at[0, n], kv_ss.at[n], kv_rs.at[n]).wait_recv()

        fw_copy(n).start()

    loop(16, forward)

    def make_keys(half, g):
        block = kvr[half, pl.ds(GROUP * g, GROUP)].reshape(SPAN, 2 * HD)
        at = pl.ds(pl.multiple_of((half * GROUP + g) * SPAN, 128), SPAN)
        kk[at, :] = jnp.concatenate([block[:, :HD], block[:, :HD]], axis=1)
        vt[:, at] = jnp.transpose(block)[HD:]

    loop(4, lambda g: make_keys(0, g))

    def partner_keys(g):
        def wait(n):
            arrival(kvr.at[1, GROUP * g + n], fw_ss.at[GROUP * g + n], fw_rs.at[GROUP * g + n]).wait_recv()

        loop(4, wait)
        make_keys(1, g)

    loop(4, partner_keys)

    def make_queries(g):
        def wait(r):
            n = GROUP * g + r

            @pl.when(n != me.e)
            def _():
                arrival(qr.at[n], q_ss.at[n], q_rs.at[n]).wait_recv()

        loop(4, wait)
        block = qr[pl.ds(GROUP * g, GROUP)].reshape(SPAN, 2 * HD)
        t = jnp.transpose(block.astype(f32)) * log2_scale
        t = jnp.concatenate([t[:HD], t[HD:]], axis=1)
        first = t.astype(bf16)
        rest = t - first.astype(f32)
        second = rest.astype(bf16)
        third = (rest - second.astype(f32)).astype(bf16)
        terms = jnp.concatenate([first, second, third, jnp.zeros_like(third)], axis=0)
        for u in range(5):
            qt[5 * g + u] = terms[:, u * TQ : (u + 1) * TQ]

    def send_back(g):
        tiles = jnp.concatenate([ot[5 * g + u] for u in range(5)], axis=1)
        heads = jnp.concatenate([tiles[:, :SPAN], tiles[:, SPAN:]], axis=0)
        atts[pl.ds(GROUP * g, GROUP)] = jnp.transpose(heads).astype(bf16).reshape(GROUP, TOK, 2 * HD)

        def send(r):
            n = GROUP * g + r

            @pl.when(n != me.e)
            def _():
                at_copy(n).start()

        loop(4, send)

    make_queries(0)
    row_top = lambda m: jnp.max(m, axis=0, keepdims=True)
    row_scale = lambda total: 1.0 / jnp.sum(total, axis=0, keepdims=True)
    s1[...] = jnp.zeros_like(s1)
    m, _, _ = attention_step(qt[0], None, None, kk, vt, s0, None, exps=False, sums=False)

    def two_tiles(p, carry):
        top, scale = carry

        @pl.when(jnp.logical_or(p == 2, jnp.logical_or(p == 4, p == 7)))
        def _():
            make_queries(lax.div(p, 2))

        @pl.when(p == 3)
        def _():
            w_arrival(1, wf.at[me.left])
            w_arrival(2, wf.at[me.right])
            for copy in w_next:
                copy.start()

        @pl.when(p == 8)
        def _():
            w_arrival(3, wf.at[me.opp, top_half])
            w_arrival(4, wf.at[me.opp, low_half])
            for copy in w_last:
                copy.start()

        m, total, out = attention_step(qt[2 * p + 1], top, scale, kk, vt, s1, s0)
        ot[jnp.maximum(2 * p - 1, 0)] = out
        top, scale = row_top(m), row_scale(total)
        m, total, out = attention_step(
            qt[jnp.minimum(2 * p + 2, TILES - 1)], top, scale, kk, vt, s0, s1
        )
        ot[2 * p] = out

        @pl.when(jnp.logical_or(p == 2, jnp.logical_or(p == 5, p == 7)))
        def _():
            send_back(lax.div(p, 3))

        return row_top(m), row_scale(total)

    _, scale = lax.fori_loop(
        0, TILES // 2, two_tiles, (row_top(m), jnp.zeros((1, TQ), f32))
    )
    _, _, out = attention_step(None, None, scale, kk, vt, s1, None, scores=False, exps=False)
    ot[TILES - 1] = out
    send_back(3)
    attr[me.head] = atts[me.e]

    w_arrival(0, wf.at[me.sib])
    other = me.sib - me.dp
    w_arrival(5, wf.at[me.left + other])
    w_arrival(6, wf.at[me.right + other])
    w_arrival(7, wf.at[me.opp + other, top_half])
    w_arrival(8, wf.at[me.opp + other, low_half])
    own_w.wait()

    def heads_in(j):
        @pl.when(j != me.head)
        def _():
            arrival(attr.at[j], at_ss.at[j], at_rs.at[j]).wait_recv()

    loop(16, heads_in)

    def project(n):
        rows = jnp.concatenate([attr[j] for j in range(KV)], axis=1)
        product = lax.dot_general(rows, wf[n], (((1,), (0,)), ((), ())), preferred_element_type=f32)
        out_ref[0, :, pl.ds(pl.multiple_of(n * W_COLS, W_COLS), W_COLS)] = product.astype(bf16)

    loop(8, project)

    def sent(n):
        @pl.when(n != me.e)
        def _():
            kv_copy(n).wait_send()
            q_copy(n).wait_send()
            at_copy(n).wait_send()

        fw_copy(n).wait_send()

    loop(16, sent)
    for copy in w_own + w_next + w_last:
        copy.wait_send()


def on_device(queries, keys, values, q_gain, k_gain, w_out):
    cos_table, sin_table = rotary_tables(lax.axis_index("sp") * TOK, TOK)
    q_gains = jnp.broadcast_to(q_gain[:, None], (HD, TOK))
    k_gains = jnp.broadcast_to(k_gain[:, None], (HD, TOK))
    dma = pltpu.SemaphoreType.DMA
    vmem = pl.BlockSpec(memory_space=pltpu.VMEM)
    return pl.pallas_call(
        layer,
        out_shape=jax.ShapeDtypeStruct((1, TOK, W_ROWS), bf16),
        in_specs=[vmem] * 8,
        out_specs=vmem,
        scratch_shapes=[
            pltpu.VMEM((16, TOK, 128), bf16),
            pltpu.VMEM((16, TOK, 128), bf16),
            pltpu.VMEM((2, 16, TOK, 128), bf16),
            pltpu.VMEM((16, TOK, 128), bf16),
            pltpu.VMEM((KEYS, 128), bf16),
            pltpu.VMEM((HD, KEYS), bf16),
            pltpu.VMEM((TILES, 256, TQ), bf16),
            pltpu.VMEM((KEYS, TQ), f32),
            pltpu.VMEM((KEYS, TQ), f32),
            pltpu.VMEM((TILES, HD, TQ), f32),
            pltpu.VMEM((16, TOK, 128), bf16),
            pltpu.VMEM((16, TOK, 128), bf16),
            pltpu.VMEM((8, W_ROWS, W_COLS), bf16),
            dma((16,)), dma((16,)), dma((16,)), dma((16,)),
            dma((16,)), dma((16,)), dma((16,)), dma((16,)),
            dma((9,)), dma((9,)), dma,
        ],
        compiler_params=pltpu.CompilerParams(
            collective_id=0, has_side_effects=True, vmem_limit_bytes=60 * 2**20
        ),
    )(queries, keys, values, w_out, cos_table, sin_table, q_gains, k_gains)


def solution(mesh):
    return jax.shard_map(
        on_device,
        mesh=mesh,
        in_specs=(P("dp", None, "sp"), P("dp", None, "sp"), P("dp", None, "sp"), P(), P(), P(None, "dp")),
        out_specs=P("dp", "sp", None),
        check_vma=False,
    )
```

time: 242 us -> 96.9 us (0.40)
  Pallas kernels: 0 us -> 87.9 us
  waiting for transfers between devices: 54.3 us -> 0 us
  blocking collectives: 46.6 us -> 0 us
  matrix products: 45.2 us -> 0 us
  other arithmetic: 33.4 us -> 1.49 us
  starting transfers between devices: 22.3 us -> 0 us
  local copies, waits for them, and re-layouts: 25 us -> 7.34 us
  between operations: 13.8 us -> 0.03 us
    pallas_call x0 -> x1, Pallas kernels: none -> 87.9 us  [on_device(): pl.pallas_call(layer, out_shape=jax.ShapeDtypeStruct((1, TOK, W_ROWS), bf...]
    all_to_all x2 -> x0, blocking collectives: 46.6 us -> none  [turned_blocks(): lax.all_to_all(parts, axes[k], split_axis=k, concat_axis=k, tiled=True)]
    dot_general x17 -> x0, matrix products: 45.2 us -> none  [the longest x8 23.6 us: one_block(): jnp.einsum('hgqk,hdk->hgdq', weights, value_heads, preferred_element_type...]
    all_to_all x3 -> x0, waiting for transfers between devices: 36.9 us -> none  [the longest x2 23.7 us: turned_blocks(): lax.all_to_all(parts, axes[k], split_axis=k, concat_axis=k, tiled=True)]
    reduce_sum x10 -> x0, other arithmetic: 20.4 us -> none  [the longest x8 18.1 us: one_block(): jnp.sum(weights, axis=-1, keepdims=True)]
    all_to_all x3 -> x0, starting transfers between devices: 19 us -> none  [the longest x1 11.6 us: sent_together(): lax.all_to_all(both, axis, split_axis=split_dim, concat_axis=concat_dim,...]
    ppermute x2 -> x0, waiting for transfers between devices: 17.3 us -> none  [swapped(): return lax.ppermute(block, axis, route)]
    reshape x6 -> x0, local copies, waits for them, and re-layouts: 7.76 us -> none  [the longest x1 2.52 us: on_device(): value_heads = value_got.reshape(kv_local, HD, seq_len)]
  transfers between devices with their start and end apart: 6 -> 0, of which waited for: 3 -> 0; matrix products, arithmetic and copies ran while one was open for 34% -> 0% of each run, Pallas kernels for 0% -> 0%
where the time goes in v1:
time: 96.9 us; the launch traced here: 96.8 us
  Pallas kernels  87.9 us (91%)
  local copies, waits for them, and re-layouts  7.34 us (8%)
  other arithmetic  1.49 us (2%)
    pallas_call x1, Pallas kernels, on_device(): pl.pallas_call(layer, out_shape=jax.ShapeDtypeStruct((1, TOK, W_ROWS), bf...  87.9 us
    unnamed x12, local copies, waits for them, and re-layouts  5.28 us

profile of v1, /device:TPU:2, one launch (start us, length us, event | category | flops | bytes accessed | tf_op | source)
XLA Modules:
  0.0 96.8 jit_solution(15925981434775621539)
XLA Ops:
  0.0 0.0 copy-start.1
  0.0 0.2 multiply_sine_fusion.1
  0.2 0.6 pad_maximum_fusion.1.sin_ref
  0.9 0.6 pad_maximum_fusion.cos_ref
  1.5 0.0 copy-start.3
  1.5 1.4 %broadcast_in_dim.4.qg_ref = f32[64,160]{1,0:T(8,128)} broadcast(f32[64]{0:T(128)} %param.9), dimensions={0} | broadcast | bytes 41216 | tf_op jit(solution)/shard_map/broadcast_in_dim | solution.py:392
  2.9 0.0 copy-done.3
  2.9 0.0 copy-start.2
  2.9 0.7 broadcast_in_dim.5.kg_ref
  3.6 0.0 copy-done.1
  3.6 0.0 copy-start
  3.6 1.0 %copy.8.k_ref = bf16[1,1024,160]{2,1,0:T(8,128)(2,1)} copy(bf16[1,1024,160]{1,2,0:T(8,128)(2,1)S(1)} %copy-done.1) | data formatting | bytes 655360 | tf_op args[1]
  4.6 0.0 copy-done.2
  4.6 1.0 %copy.9.v_ref = bf16[1,1024,160]{2,1,0:T(8,128)(2,1)} copy(bf16[1,1024,160]{1,2,0:T(8,128)(2,1)S(1)} %copy-done.2) | data formatting | bytes 655360 | tf_op args[2]
  5.6 0.0 copy-done
  5.6 1.3 %copy.7.q_ref = bf16[1,2048,160]{2,1,0:T(8,128)(2,1)} copy(bf16[1,2048,160]{1,2,0:T(8,128)(2,1)S(1)} %copy-done) | data formatting | bytes 1310720 | tf_op args[0]
  6.9 87.9 %shard_map.64 = bf16[1,160,2048]{2,1,0:T(8,128)(2,1)} custom-call(bf16[1,2048,160]{2,1,0:T(8,128)(2,1)} %copy.7.q_ref, bf16[1,1024,160]{2,1,0:T(8,128)(2,1)} %copy.8.k_ref, bf16[1,1024,160]{2,1,0:T(8,128)(2,1)} %copy.9.v_ref, bf16[2048,256]{1,0:T(8,128)(2,1)} %w_ref.1, f32[64,160]{1,0:T(8,128)} %pad_maximum_fusion.cos_ref, ...), custom_call_target="tpu_custom_call" | custom-call | tf_op jit(solution)/shard_map/pallas_call | solution.py:396
  94.8 2.0 %copy.11 = bf16[1,160,2048]{2,1,0:T(8,128)(2,1)} copy(bf16[1,160,2048]{2,1,0:T(8,128)(2,1)} %shard_map.64) | data formatting | bytes 1310720
  (2 shorter events, 0.0 us)
Async XLA Ops:
  0.0 3.6 %copy-start.1 = (bf16[1,1024,160]{1,2,0:T(8,128)(2,1)S(1)}, bf16[1,1024,160]{1,2,0:T(8,128)(2,1)}, u32[]{:S(2)}) copy-start(bf16[1,1024,160]{1,2,0:T(8,128)(2,1)} %param.7) | copy-start | bytes 983044
  1.5 1.4 %copy-start.3 = (f32[64]{0:T(128)S(1)}, f32[64]{0:T(128)}, u32[]{:S(2)}) copy-start(f32[64]{0:T(128)} %param.10) | copy-start | bytes 772
  2.9 1.7 %copy-start.2 = (bf16[1,1024,160]{1,2,0:T(8,128)(2,1)S(1)}, bf16[1,1024,160]{1,2,0:T(8,128)(2,1)}, u32[]{:S(2)}) copy-start(bf16[1,1024,160]{1,2,0:T(8,128)(2,1)} %param.8) | copy-start | bytes 983044
  3.6 2.0 %copy-start = (bf16[1,2048,160]{1,2,0:T(8,128)(2,1)S(1)}, bf16[1,2048,160]{1,2,0:T(8,128)(2,1)}, u32[]{:S(2)}) copy-start(bf16[1,2048,160]{1,2,0:T(8,128)(2,1)} %param.6) | copy-start | bytes 1966084

commit v2 on v1

--- a/solution.py
+++ b/solution.py
@@ -23,35 +23,44 @@
 W_COLS = 256
 
 epsilon = 1e-06
-rotary_base = 10000.0
+octaves = -13.287712379549449 / 16
 log2_scale = HD ** (-0.5) * 1.4426950408889634
 f32 = jnp.float32
 bf16 = jnp.bfloat16
 MESH = pl.DeviceIdType.MESH
 
 
-def rotary_tables(first_row, row_count):
-    position = first_row + lax.iota(jnp.int32, row_count)
-    grid_row = (position // GRID_W).astype(f32)
-    grid_col = (position % GRID_W).astype(f32)
-    quarter = HD // 4
-    inv_freq = rotary_base ** (-(2.0 * lax.iota(f32, quarter)) / (HD // 2))
-    row_angle = inv_freq[:, None] * grid_row[None, :]
-    col_angle = inv_freq[:, None] * grid_col[None, :]
-    cos_table = jnp.concatenate(
-        [jnp.cos(row_angle), jnp.cos(row_angle), jnp.cos(col_angle), jnp.cos(col_angle)], axis=0
-    )
-    sin_table = jnp.concatenate(
-        [jnp.sin(row_angle), jnp.sin(row_angle), jnp.sin(col_angle), jnp.sin(col_angle)], axis=0
-    )
-    return (cos_table, sin_table)
-
-
-def turned(field, gain, cos_table, sin_table):
-    u = field.astype(f32)
-    n = u * lax.rsqrt(jnp.mean(u * u, axis=0, keepdims=True) + epsilon) * gain
-    rot = jnp.concatenate([-n[16:32], n[0:16], -n[48:64], n[32:48]], axis=0)
-    return n * cos_table + rot * sin_table
+def lanes(rows):
+    return lax.broadcasted_iota(jnp.int32, (rows, 2 * HD), 1)
+
+
+def rotary_tables(first_row):
+    lane = lanes(TOK)
+    position = first_row + lax.broadcasted_iota(jnp.int32, (TOK, 2 * HD), 0)
+    place = jnp.where((lane & 32) == 0, position >> 6, position & (GRID_W - 1)).astype(f32)
+    angle = place * jnp.exp2((lane & 15).astype(f32) * octaves)
+    sin_table = jnp.sin(angle)
+    return jnp.cos(angle), jnp.where((lane & 16) == 0, -sin_table, sin_table)
+
+
+def head_sums():
+    row = lax.broadcasted_iota(jnp.int32, (4 * HD, 2 * HD), 0)
+    col = lax.broadcasted_iota(jnp.int32, (4 * HD, 2 * HD), 1)
+    return jnp.where(((row >> 6) & 1) == (col >> 6), 1.0, 0.0).astype(bf16)
+
+
+def turned(u, gain, tables, ones):
+    square = u * u
+    high = square.astype(bf16)
+    low = (square - high.astype(f32)).astype(bf16)
+    sums = lax.dot_general(
+        jnp.concatenate([high, low], axis=1), ones, (((1,), (0,)), ((), ())), preferred_element_type=f32
+    )
+    n = u * lax.rsqrt(sums * (1.0 / HD) + epsilon) * gain
+    rot = jnp.where(
+        (lanes(TOK) & 16) == 0, pltpu.roll(n, 2 * HD - 16, 1), pltpu.roll(n, 16, 1)
+    )
+    return n * tables[0] + rot * tables[1]
 
 
 class Place:
@@ -62,6 +71,7 @@
         self.g = lax.div(self.y, 2)
         self.e = self.g * (3 - self.y) + (1 - self.g) * self.y
         self.head = 2 * self.z + self.e
+        self.own = 12 + self.e
         self.partner = self.z * Y + 3 - self.y
         x, self.c = lax.div(self.dp, 2), lax.rem(self.dp, 2)
         self.left = lax.rem(x + X - 1, X) * 2 + self.c
@@ -70,7 +80,7 @@
         self.opp = lax.rem(x + 2, X) * 2 + self.c
 
     def offset(self, n):
-        i = lax.div(n, 2)
+        i = lax.rem(lax.div(n, 2) + 2, Z)
         return lax.div(i + 1, 2) * (2 * lax.rem(i, 2) - 1)
 
     def at(self, z, e):
@@ -94,34 +104,42 @@
     lax.fori_loop(0, count, step, 0)
 
 
-def attention_step(q, top, scale, kk, vt, x_ref, y_ref, scores=True, exps=True, sums=True):
+def scores_of(k, q):
+    return lax.dot_general(k, q, (((1,), (0,)), ((), ())), preferred_element_type=f32)
+
+
+def by_eight(x):
+    return x.reshape(x.shape[0] // 8, 8, TQ)
+
+
+def attention_step(q, top, scale, kk, vt, x_ref, y_ref, scores=True, exps=True):
     m = jnp.full((8, TQ), -jnp.inf, f32)
     total = jnp.zeros((8, TQ), f32)
     out = None
+    tops = jnp.broadcast_to(top, (8, TQ)) if exps else None
+    scales = jnp.broadcast_to(scale, (8, TQ))
+    zeros = []
     for j in range(KEYS // KC):
         at = slice(j * KC, (j + 1) * KC)
-        if sums:
-            weights = (x_ref[at, :] * scale).astype(bf16)
-            part = lax.dot_general(
-                vt[:, at], weights, (((1,), (0,)), ((), ())), preferred_element_type=f32
-            )
-            out = part if out is None else out + part
+        if exps:
+            e = jnp.exp2(by_eight(y_ref[at, :]) - tops)
+            y_ref[at, :] = e.reshape(KC, TQ)
+            part = jnp.sum(e, axis=0)
+            total = total + part
+            zeros.append(jnp.minimum(part, 0.0))
+        by = scales + zeros[j - 2] if exps and j >= 2 else scales
+        weights = (by_eight(x_ref[at, :]) * by).reshape(KC, TQ).astype(bf16)
+        part = lax.dot_general(vt[:, at], weights, (((1,), (0,)), ((), ())), preferred_element_type=f32)
+        out = part if out is None else out + part
         if scores:
-            k = kk[at, :]
-            s = lax.dot_general(
-                jnp.concatenate([k, k], axis=1), q, (((1,), (0,)), ((), ())), preferred_element_type=f32
-            )
+            s = scores_of(kk[at, :], q)
             x_ref[at, :] = s
-            m = jnp.maximum(m, jnp.max(s.reshape(KC // 8, 8, TQ), axis=0))
-        if exps:
-            e = jnp.exp2(y_ref[at, :] - top)
-            y_ref[at, :] = e
-            total = total + jnp.sum(e.reshape(KC // 8, 8, TQ), axis=0)
+            m = jnp.maximum(m, jnp.max(by_eight(s), axis=0))
     return m, total, out
 
 
 def layer(
-    q_ref, k_ref, v_ref, w_ref, cos_ref, sin_ref, qg_ref, kg_ref, out_ref,
+    q_ref, k_ref, v_ref, w_ref, qg_ref, kg_ref, out_ref,
     kvs, qs, kvr, qr, kk, vt, qt, s0, s1, ot, atts, attr, wf,
     kv_ss, kv_rs, fw_ss, fw_rs, q_ss, q_rs, at_ss, at_rs, w_ss, w_rs, own_sem,
 ):
@@ -138,7 +156,7 @@
         pl.semaphore_signal(barrier, inc=1, device_id=device, device_id_type=MESH)
 
     def greet(n):
-        @pl.when(n != me.e)
+        @pl.when(n != me.own)
         def _():
             hello(sp=me.at(me.target_z(n), lax.rem(n, 2)))
 
@@ -148,24 +166,27 @@
     hello(dp=me.left)
     hello(dp=me.right)
 
-    cos_table, sin_table = cos_ref[...], sin_ref[...]
-
-    def make_kv(n):
-        j = 2 * me.target_z(n) + lax.rem(n, 2)
-        rows = pl.ds(pl.multiple_of(j * HD, HD), HD)
-        k = turned(k_ref[0, rows, :], kg_ref[...], cos_table, sin_table)
-        both = jnp.concatenate([k, v_ref[0, rows, :].astype(f32)], axis=0)
-        kvs[n] = jnp.transpose(both).astype(bf16)
+    tables = rotary_tables(lax.axis_index("sp") * TOK)
+    ones = head_sums()
+
+    def two_heads(ref):
+        gain = ref[...].reshape(1, HD)
+        return jnp.concatenate([gain, gain], axis=1)
+
+    q_gain, k_gain = two_heads(qg_ref), two_heads(kg_ref)
+    first_head = lanes(TOK) < HD
+
+    def make_kv(i):
+        at = pl.ds(pl.multiple_of(me.target_z(2 * i) * 2 * HD, 2 * HD), 2 * HD)
+        k = turned(k_ref[0, :, at].astype(f32), k_gain, tables, ones)
+        v = v_ref[0, :, at].astype(f32)
+        kvs[2 * i] = jnp.where(first_head, k, pltpu.roll(v, HD, 1)).astype(bf16)
+        kvs[2 * i + 1] = jnp.where(first_head, pltpu.roll(k, HD, 1), v).astype(bf16)
 
     def make_q(n):
         j = 2 * me.target_z(n) + lax.rem(n, 2)
-        a = q_ref[0, pl.ds(pl.multiple_of(j * 2 * HD, HD), HD), :]
-        b = q_ref[0, pl.ds(pl.multiple_of(j * 2 * HD + HD, HD), HD), :]
-        both = jnp.concatenate(
-            [turned(a, qg_ref[...], cos_table, sin_table), turned(b, qg_ref[...], cos_table, sin_table)],
-            axis=0,
-        )
-        qs[n] = jnp.transpose(both).astype(bf16)
+        at = pl.ds(pl.multiple_of(j * 2 * HD, 2 * HD), 2 * HD)
+        qs[n] = turned(q_ref[0, :, at].astype(f32), q_gain, tables, ones).astype(bf16)
 
     def kv_copy(n):
         there = me.slot_there(n)
@@ -217,33 +238,41 @@
     def w_arrival(kind, ref):
         arrival(ref, w_ss.at[kind], w_rs.at[kind]).wait_recv()
 
-    loop(16, make_kv)
+    def make_four(r):
+        make_kv(2 * r)
+        make_kv(2 * r + 1)
+
+    loop(4, make_four)
     pl.semaphore_wait(barrier, 19)
 
     def send_kv(n):
-        @pl.when(n != me.e)
+        @pl.when(n != me.own)
         def _():
             kv_copy(n).start()
 
-        make_q(n)
-
     loop(16, send_kv)
+    kvr[0, me.own] = kvs[me.own]
+
+    def make_q_four(r):
+        for n in range(4):
+            make_q(4 * r + n)
+
+    loop(4, make_q_four)
 
     def send_q(n):
-        @pl.when(n != me.e)
+        @pl.when(n != me.own)
         def _():
             q_copy(n).start()
 
     loop(16, send_q)
+    qr[me.own] = qs[me.own]
     own_w = pltpu.make_async_copy(w_ref, wf.at[me.dp], own_sem)
     own_w.start()
     for copy in w_own:
         copy.start()
-    kvr[0, me.e] = kvs[me.e]
-    qr[me.e] = qs[me.e]
 
     def forward(n):
-        @pl.when(n != me.e)
+        @pl.when(n != me.own)
         def _():
             arrival(kvr.at[0, n], kv_ss.at[n], kv_rs.at[n]).wait_recv()
 
@@ -254,25 +283,16 @@
     def make_keys(half, g):
         block = kvr[half, pl.ds(GROUP * g, GROUP)].reshape(SPAN, 2 * HD)
         at = pl.ds(pl.multiple_of((half * GROUP + g) * SPAN, 128), SPAN)
-        kk[at, :] = jnp.concatenate([block[:, :HD], block[:, :HD]], axis=1)
+        twice = jnp.concatenate([block[:, :HD], block[:, :HD]], axis=1)
+        kk[at, :] = twice
         vt[:, at] = jnp.transpose(block)[HD:]
-
-    loop(4, lambda g: make_keys(0, g))
-
-    def partner_keys(g):
-        def wait(n):
-            arrival(kvr.at[1, GROUP * g + n], fw_ss.at[GROUP * g + n], fw_rs.at[GROUP * g + n]).wait_recv()
-
-        loop(4, wait)
-        make_keys(1, g)
-
-    loop(4, partner_keys)
+        return at, twice
 
     def make_queries(g):
         def wait(r):
             n = GROUP * g + r
 
-            @pl.when(n != me.e)
+            @pl.when(n != me.own)
             def _():
                 arrival(qr.at[n], q_ss.at[n], q_rs.at[n]).wait_recv()
 
@@ -281,10 +301,8 @@
         t = jnp.transpose(block.astype(f32)) * log2_scale
         t = jnp.concatenate([t[:HD], t[HD:]], axis=1)
         first = t.astype(bf16)
-        rest = t - first.astype(f32)
-        second = rest.astype(bf16)
-        third = (rest - second.astype(f32)).astype(bf16)
-        terms = jnp.concatenate([first, second, third, jnp.zeros_like(third)], axis=0)
+        second = (t - first.astype(f32)).astype(bf16)
+        terms = jnp.concatenate([first, second], axis=0)
         for u in range(5):
             qt[5 * g + u] = terms[:, u * TQ : (u + 1) * TQ]
 
@@ -296,17 +314,33 @@
         def send(r):
             n = GROUP * g + r
 
-            @pl.when(n != me.e)
+            @pl.when(n != me.own)
             def _():
                 at_copy(n).start()
 
         loop(4, send)
 
-    make_queries(0)
     row_top = lambda m: jnp.max(m, axis=0, keepdims=True)
     row_scale = lambda total: 1.0 / jnp.sum(total, axis=0, keepdims=True)
     s1[...] = jnp.zeros_like(s1)
-    m, _, _ = attention_step(qt[0], None, None, kk, vt, s0, None, exps=False, sums=False)
+    make_queries(0)
+
+    def first_scores(half, g, m):
+        at, twice = make_keys(half, g)
+        s = scores_of(twice, qt[0])
+        s0[at, :] = s
+        return jnp.maximum(m, jnp.max(by_eight(s), axis=0))
+
+    def partner_keys(g, m):
+        def wait(n):
+            arrival(kvr.at[1, GROUP * g + n], fw_ss.at[GROUP * g + n], fw_rs.at[GROUP * g + n]).wait_recv()
+
+        loop(4, wait)
+        return first_scores(1, g, m)
+
+    m = jnp.full((8, TQ), -jnp.inf, f32)
+    m = lax.fori_loop(0, 4, lambda g, m: first_scores(0, g, m), m)
+    m = lax.fori_loop(0, 4, partner_keys, m)
 
     def two_tiles(p, carry):
         top, scale = carry
@@ -349,7 +383,7 @@
     _, _, out = attention_step(None, None, scale, kk, vt, s1, None, scores=False, exps=False)
     ot[TILES - 1] = out
     send_back(3)
-    attr[me.head] = atts[me.e]
+    attr[me.head] = atts[me.own]
 
     w_arrival(0, wf.at[me.sib])
     other = me.sib - me.dp
@@ -374,7 +408,7 @@
     loop(8, project)
 
     def sent(n):
-        @pl.when(n != me.e)
+        @pl.when(n != me.own)
         def _():
             kv_copy(n).wait_send()
             q_copy(n).wait_send()
@@ -388,15 +422,12 @@
 
 
 def on_device(queries, keys, values, q_gain, k_gain, w_out):
-    cos_table, sin_table = rotary_tables(lax.axis_index("sp") * TOK, TOK)
-    q_gains = jnp.broadcast_to(q_gain[:, None], (HD, TOK))
-    k_gains = jnp.broadcast_to(k_gain[:, None], (HD, TOK))
     dma = pltpu.SemaphoreType.DMA
     vmem = pl.BlockSpec(memory_space=pltpu.VMEM)
     return pl.pallas_call(
         layer,
         out_shape=jax.ShapeDtypeStruct((1, TOK, W_ROWS), bf16),
-        in_specs=[vmem] * 8,
+        in_specs=[vmem] * 6,
         out_specs=vmem,
         scratch_shapes=[
             pltpu.VMEM((16, TOK, 128), bf16),
@@ -405,7 +436,7 @@
             pltpu.VMEM((16, TOK, 128), bf16),
             pltpu.VMEM((KEYS, 128), bf16),
             pltpu.VMEM((HD, KEYS), bf16),
-            pltpu.VMEM((TILES, 256, TQ), bf16),
+            pltpu.VMEM((TILES, 2 * HD, TQ), bf16),
             pltpu.VMEM((KEYS, TQ), f32),
             pltpu.VMEM((KEYS, TQ), f32),
             pltpu.VMEM((TILES, HD, TQ), f32),
@@ -419,7 +450,14 @@
         compiler_params=pltpu.CompilerParams(
             collective_id=0, has_side_effects=True, vmem_limit_bytes=60 * 2**20
         ),
-    )(queries, keys, values, w_out, cos_table, sin_table, q_gains, k_gains)
+    )(
+        jnp.swapaxes(queries, 1, 2),
+        jnp.swapaxes(keys, 1, 2),
+        jnp.swapaxes(values, 1, 2),
+        w_out,
+        q_gain,
+        k_gain,
+    )
 
 
 def solution(mesh):

time: 96.9 us -> 81.1 us (0.84)
  Pallas kernels: 87.9 us -> 78.6 us
  local copies, waits for them, and re-layouts: 7.34 us -> 1.98 us
  other arithmetic: 1.49 us -> 0 us
    pallas_call x1, Pallas kernels: 87.9 us -> 78.6 us  [on_device(): pl.pallas_call(layer, out_shape=jax.ShapeDtypeStruct((1, TOK, W_ROWS), bf...]
    unnamed x12 -> x1, local copies, waits for them, and re-layouts: 5.28 us -> 1.98 us
    broadcast_in_dim x2 -> x0, local copies, waits for them, and re-layouts: 2.06 us -> none  [the longest x1 1.36 us: on_device(): q_gains = jnp.broadcast_to(q_gain[:, None], (HD, TOK))]
    concatenate x2 -> x0, other arithmetic: 1.27 us -> none  [the longest x1 0.64 us: rotary_tables(): jnp.concatenate([jnp.sin(row_angle), jnp.sin(row_angle), jnp.sin(col_angl...]
where the time goes in v2:
time: 81.1 us; the launch traced here: 80.5 us
  Pallas kernels  78.6 us (97%)
  local copies, waits for them, and re-layouts  1.98 us (2%)
    pallas_call x1, Pallas kernels, on_device(): pl.pallas_call(layer, out_shape=jax.ShapeDtypeStruct((1, TOK, W_ROWS), bf...  78.6 us
    unnamed x1, local copies, waits for them, and re-layouts  1.98 us

profile of v2, /device:TPU:2, one launch (start us, length us, event | category | flops | bytes accessed | tf_op | source)
XLA Modules:
  0.0 80.5 jit_solution(2496907232095979519)
XLA Ops:
  0.0 78.6 %shard_map.64 = bf16[1,160,2048]{2,1,0:T(8,128)(2,1)} custom-call(bf16[1,160,2048]{2,1,0:T(8,128)(2,1)} %bitcast.3, bf16[1,160,1024]{2,1,0:T(8,128)(2,1)} %bitcast.4, bf16[1,160,1024]{2,1,0:T(8,128)(2,1)} %bitcast.5, bf16[2048,256]{1,0:T(8,128)(2,1)} %w_ref.1, f32[64]{0:T(128)} %qg_ref.1, f32[64]{0:T(128)} %kg_ref.1), custom_call_target="tpu_custom_call" | custom-call | tf_op jit(solution)/shard_map/pallas_call | solution.py:427
  78.6 2.0 %copy.8 = bf16[1,160,2048]{2,1,0:T(8,128)(2,1)} copy(bf16[1,160,2048]{2,1,0:T(8,128)(2,1)} %shard_map.64) | data formatting | bytes 1310720

commit v3 on v2

--- a/solution.py
+++ b/solution.py
@@ -63,6 +63,14 @@
     return n * tables[0] + rot * tables[1]
 
 
+def div(a, b):
+    return a // b if isinstance(a, int) else lax.div(a, b)
+
+
+def rem(a, b):
+    return a % b if isinstance(a, int) else lax.rem(a, b)
+
+
 class Place:
     def __init__(self):
         sp = lax.axis_index("sp")
@@ -80,8 +88,8 @@
         self.opp = lax.rem(x + 2, X) * 2 + self.c
 
     def offset(self, n):
-        i = lax.rem(lax.div(n, 2) + 2, Z)
-        return lax.div(i + 1, 2) * (2 * lax.rem(i, 2) - 1)
+        i = rem(div(n, 2) + 2, Z)
+        return div(i + 1, 2) * (2 * rem(i, 2) - 1)
 
     def at(self, z, e):
         return z * Y + self.g * 3 + e * (1 - 2 * self.g)
@@ -93,7 +101,15 @@
         return lax.rem(self.z - self.offset(n) + Z, Z)
 
     def slot_there(self, n):
-        return 2 * lax.div(n, 2) + self.e
+        return 2 * div(n, 2) + self.e
+
+
+def all_slots(me, body):
+    for n in range(16):
+        if n in (12, 13):
+            pl.when(n != me.own)(lambda n=n: body(n))
+        else:
+            body(n)
 
 
 def loop(count, body):
@@ -142,6 +158,7 @@
     q_ref, k_ref, v_ref, w_ref, qg_ref, kg_ref, out_ref,
     kvs, qs, kvr, qr, kk, vt, qt, s0, s1, ot, atts, attr, wf,
     kv_ss, kv_rs, fw_ss, fw_rs, q_ss, q_rs, at_ss, at_rs, w_ss, w_rs, own_sem,
+    k_in, v_in, q_in, in_sem,
 ):
     me = Place()
 
@@ -155,12 +172,13 @@
     def hello(**device):
         pl.semaphore_signal(barrier, inc=1, device_id=device, device_id_type=MESH)
 
-    def greet(n):
-        @pl.when(n != me.own)
-        def _():
-            hello(sp=me.at(me.target_z(n), lax.rem(n, 2)))
-
-    loop(16, greet)
+    inputs = [
+        pltpu.make_async_copy(src.at[0], dst, in_sem.at[n])
+        for n, (src, dst) in enumerate(((k_ref, k_in), (v_ref, v_in), (q_ref, q_in)))
+    ]
+    for copy in inputs:
+        copy.start()
+    all_slots(me, lambda n: hello(sp=me.at(me.target_z(n), rem(n, 2))))
     hello(sp=me.partner)
     hello(dp=me.sib)
     hello(dp=me.left)
@@ -178,28 +196,28 @@
 
     def make_kv(i):
         at = pl.ds(pl.multiple_of(me.target_z(2 * i) * 2 * HD, 2 * HD), 2 * HD)
-        k = turned(k_ref[0, :, at].astype(f32), k_gain, tables, ones)
-        v = v_ref[0, :, at].astype(f32)
+        k = turned(k_in[:, at].astype(f32), k_gain, tables, ones)
+        v = v_in[:, at].astype(f32)
         kvs[2 * i] = jnp.where(first_head, k, pltpu.roll(v, HD, 1)).astype(bf16)
         kvs[2 * i + 1] = jnp.where(first_head, pltpu.roll(k, HD, 1), v).astype(bf16)
 
     def make_q(n):
-        j = 2 * me.target_z(n) + lax.rem(n, 2)
+        j = 2 * me.target_z(n) + rem(n, 2)
         at = pl.ds(pl.multiple_of(j * 2 * HD, 2 * HD), 2 * HD)
-        qs[n] = turned(q_ref[0, :, at].astype(f32), q_gain, tables, ones).astype(bf16)
+        qs[n] = turned(q_in[:, at].astype(f32), q_gain, tables, ones).astype(bf16)
 
     def kv_copy(n):
         there = me.slot_there(n)
         return remote(
             kvs.at[n], kvr.at[0, there], kv_ss.at[n], kv_rs.at[there],
-            sp=me.at(me.target_z(n), lax.rem(n, 2)),
+            sp=me.at(me.target_z(n), rem(n, 2)),
         )
 
     def q_copy(n):
         there = me.slot_there(n)
         return remote(
             qs.at[n], qr.at[there], q_ss.at[n], q_rs.at[there],
-            sp=me.at(me.target_z(n), lax.rem(n, 2)),
+            sp=me.at(me.target_z(n), rem(n, 2)),
         )
 
     def fw_copy(n):
@@ -208,7 +226,7 @@
     def at_copy(n):
         return remote(
             atts.at[n], attr.at[me.head], at_ss.at[n], at_rs.at[me.head],
-            sp=me.at(me.source_z(n), lax.rem(n, 2)),
+            sp=me.at(me.source_z(n), rem(n, 2)),
         )
 
     def arrival(ref, ss, rs):
@@ -242,29 +260,22 @@
         make_kv(2 * r)
         make_kv(2 * r + 1)
 
+    inputs[0].wait()
+    inputs[1].wait()
     loop(4, make_four)
     pl.semaphore_wait(barrier, 19)
 
-    def send_kv(n):
-        @pl.when(n != me.own)
-        def _():
-            kv_copy(n).start()
-
-    loop(16, send_kv)
+    all_slots(me, lambda n: kv_copy(n).start())
     kvr[0, me.own] = kvs[me.own]
 
     def make_q_four(r):
         for n in range(4):
             make_q(4 * r + n)
 
+    inputs[2].wait()
     loop(4, make_q_four)
 
-    def send_q(n):
-        @pl.when(n != me.own)
-        def _():
-            q_copy(n).start()
-
-    loop(16, send_q)
+    all_slots(me, lambda n: q_copy(n).start())
     qr[me.own] = qs[me.own]
     own_w = pltpu.make_async_copy(w_ref, wf.at[me.dp], own_sem)
     own_w.start()
@@ -349,6 +360,10 @@
         def _():
             make_queries(lax.div(p, 2))
 
+        m, total, out = attention_step(qt[2 * p + 1], top, scale, kk, vt, s1, s0)
+        ot[jnp.maximum(2 * p - 1, 0)] = out
+        top, scale = row_top(m), row_scale(total)
+
         @pl.when(p == 3)
         def _():
             w_arrival(1, wf.at[me.left])
@@ -363,9 +378,6 @@
             for copy in w_last:
                 copy.start()
 
-        m, total, out = attention_step(qt[2 * p + 1], top, scale, kk, vt, s1, s0)
-        ot[jnp.maximum(2 * p - 1, 0)] = out
-        top, scale = row_top(m), row_scale(total)
         m, total, out = attention_step(
             qt[jnp.minimum(2 * p + 2, TILES - 1)], top, scale, kk, vt, s0, s1
         )
@@ -424,10 +436,11 @@
 def on_device(queries, keys, values, q_gain, k_gain, w_out):
     dma = pltpu.SemaphoreType.DMA
     vmem = pl.BlockSpec(memory_space=pltpu.VMEM)
+    anywhere = pl.BlockSpec(memory_space=pl.ANY)
     return pl.pallas_call(
         layer,
         out_shape=jax.ShapeDtypeStruct((1, TOK, W_ROWS), bf16),
-        in_specs=[vmem] * 6,
+        in_specs=[anywhere] * 4 + [vmem] * 2,
         out_specs=vmem,
         scratch_shapes=[
             pltpu.VMEM((16, TOK, 128), bf16),
@@ -446,6 +459,10 @@
             dma((16,)), dma((16,)), dma((16,)), dma((16,)),
             dma((16,)), dma((16,)), dma((16,)), dma((16,)),
             dma((9,)), dma((9,)), dma,
+            pltpu.VMEM((TOK, KV * HD), bf16),
+            pltpu.VMEM((TOK, KV * HD), bf16),
+            pltpu.VMEM((TOK, QH * HD), bf16),
+            dma((3,)),
         ],
         compiler_params=pltpu.CompilerParams(
             collective_id=0, has_side_effects=True, vmem_limit_bytes=60 * 2**20

time: 81.1 us -> 76.5 us (0.943)
  Pallas kernels: 78.6 us -> 74.3 us
    pallas_call x1, Pallas kernels: 78.6 us -> 74.3 us  [on_device(): pl.pallas_call(layer, out_shape=jax.ShapeDtypeStruct((1, TOK, W_ROWS), bf...]
where the time goes in v3:
time: 76.5 us; the launch traced here: 76.3 us
  Pallas kernels  74.3 us (97%)
  local copies, waits for them, and re-layouts  1.98 us (3%)
    pallas_call x1, Pallas kernels, on_device(): pl.pallas_call(layer, out_shape=jax.ShapeDtypeStruct((1, TOK, W_ROWS), bf...  74.3 us
    unnamed x1, local copies, waits for them, and re-layouts  1.98 us

profile of v3, /device:TPU:2, one launch (start us, length us, event | category | flops | bytes accessed | tf_op | source)
XLA Modules:
  0.0 76.3 jit_solution(17775758384376885501)
XLA Ops:
  0.0 74.3 %shard_map.64 = bf16[1,160,2048]{2,1,0:T(8,128)(2,1)} custom-call(bf16[1,160,2048]{2,1,0:T(8,128)(2,1)} %bitcast.3, bf16[1,160,1024]{2,1,0:T(8,128)(2,1)} %bitcast.4, bf16[1,160,1024]{2,1,0:T(8,128)(2,1)} %bitcast.5, bf16[2048,256]{1,0:T(8,128)(2,1)} %w_ref.1, f32[64]{0:T(128)} %qg_ref.1, f32[64]{0:T(128)} %kg_ref.1), custom_call_target="tpu_custom_call" | custom-call | tf_op jit(solution)/shard_map/pallas_call | solution.py:440
  74.3 2.0 %copy.8 = bf16[1,160,2048]{2,1,0:T(8,128)(2,1)} copy(bf16[1,160,2048]{2,1,0:T(8,128)(2,1)} %shard_map.64) | data formatting | bytes 1310720

commit v4 on v3

--- a/solution.py
+++ b/solution.py
@@ -397,6 +397,19 @@
     send_back(3)
     attr[me.head] = atts[me.own]
 
+    def sent(n):
+        @pl.when(n != me.own)
+        def _():
+            kv_copy(n).wait_send()
+            q_copy(n).wait_send()
+
+        fw_copy(n).wait_send()
+
+    loop(16, sent)
+    loop(12, lambda n: at_copy(n).wait_send())
+    for copy in w_own + w_next + w_last:
+        copy.wait_send()
+
     w_arrival(0, wf.at[me.sib])
     other = me.sib - me.dp
     w_arrival(5, wf.at[me.left + other])
@@ -419,18 +432,11 @@
 
     loop(8, project)
 
-    def sent(n):
-        @pl.when(n != me.own)
-        def _():
-            kv_copy(n).wait_send()
-            q_copy(n).wait_send()
+    for n in range(12, 16):
+        if n < 14:
+            pl.when(n != me.own)(lambda n=n: at_copy(n).wait_send())
+        else:
             at_copy(n).wait_send()
-
-        fw_copy(n).wait_send()
-
-    loop(16, sent)
-    for copy in w_own + w_next + w_last:
-        copy.wait_send()
 
 
 def on_device(queries, keys, values, q_gain, k_gain, w_out):

time: 76.5 us -> 76.3 us (level)
  no operation moved by 1% of the time
where the time goes in v4:
time: 76.3 us; the launch traced here: 76.1 us
  Pallas kernels  74.1 us (97%)
  local copies, waits for them, and re-layouts  1.98 us (3%)
    pallas_call x1, Pallas kernels, on_device(): pl.pallas_call(layer, out_shape=jax.ShapeDtypeStruct((1, TOK, W_ROWS), bf...  74.1 us
    unnamed x1, local copies, waits for them, and re-layouts  1.98 us

profile of v4, /device:TPU:2, one launch (start us, length us, event | category | flops | bytes accessed | tf_op | source)
XLA Modules:
  0.0 76.1 jit_solution(2569657668636039759)
XLA Ops:
  0.0 74.1 %shard_map.64 = bf16[1,160,2048]{2,1,0:T(8,128)(2,1)} custom-call(bf16[1,160,2048]{2,1,0:T(8,128)(2,1)} %bitcast.3, bf16[1,160,1024]{2,1,0:T(8,128)(2,1)} %bitcast.4, bf16[1,160,1024]{2,1,0:T(8,128)(2,1)} %bitcast.5, bf16[2048,256]{1,0:T(8,128)(2,1)} %w_ref.1, f32[64]{0:T(128)} %qg_ref.1, f32[64]{0:T(128)} %kg_ref.1), custom_call_target="tpu_custom_call" | custom-call | tf_op jit(solution)/shard_map/pallas_call | solution.py:446
  74.1 2.0 %copy.8 = bf16[1,160,2048]{2,1,0:T(8,128)(2,1)} copy(bf16[1,160,2048]{2,1,0:T(8,128)(2,1)} %shard_map.64) | data formatting | bytes 1310720

commit v5 on v4

--- a/solution.py
+++ b/solution.py
@@ -289,7 +289,6 @@
 
         fw_copy(n).start()
 
-    loop(16, forward)
 
     def make_keys(half, g):
         block = kvr[half, pl.ds(GROUP * g, GROUP)].reshape(SPAN, 2 * HD)
@@ -297,7 +296,6 @@
         twice = jnp.concatenate([block[:, :HD], block[:, :HD]], axis=1)
         kk[at, :] = twice
         vt[:, at] = jnp.transpose(block)[HD:]
-        return at, twice
 
     def make_queries(g):
         def wait(r):
@@ -334,11 +332,17 @@
     row_top = lambda m: jnp.max(m, axis=0, keepdims=True)
     row_scale = lambda total: 1.0 / jnp.sum(total, axis=0, keepdims=True)
     s1[...] = jnp.zeros_like(s1)
+
+    def own_keys(g):
+        loop(GROUP, lambda r: forward(GROUP * g + r))
+        make_keys(0, g)
+
+    loop(4, own_keys)
     make_queries(0)
 
     def first_scores(half, g, m):
-        at, twice = make_keys(half, g)
-        s = scores_of(twice, qt[0])
+        at = pl.ds(pl.multiple_of((half * GROUP + g) * SPAN, 128), SPAN)
+        s = scores_of(kk[at, :], qt[0])
         s0[at, :] = s
         return jnp.maximum(m, jnp.max(by_eight(s), axis=0))
 
@@ -347,6 +351,7 @@
             arrival(kvr.at[1, GROUP * g + n], fw_ss.at[GROUP * g + n], fw_rs.at[GROUP * g + n]).wait_recv()
 
         loop(4, wait)
+        make_keys(1, g)
         return first_scores(1, g, m)
 
     m = jnp.full((8, TQ), -jnp.inf, f32)

time: 76.3 us -> 76.2 us (level)
  no operation moved by 1% of the time
where the time goes in v5:
time: 76.2 us; the launch traced here: 76.1 us
  Pallas kernels  74.1 us (97%)
  local copies, waits for them, and re-layouts  1.98 us (3%)
    pallas_call x1, Pallas kernels, on_device(): pl.pallas_call(layer, out_shape=jax.ShapeDtypeStruct((1, TOK, W_ROWS), bf...  74.1 us
    unnamed x1, local copies, waits for them, and re-layouts  1.98 us

profile of v5, /device:TPU:2, one launch (start us, length us, event | category | flops | bytes accessed | tf_op | source)
XLA Modules:
  0.0 76.1 jit_solution(6443757696493853352)
XLA Ops:
  0.0 74.1 %shard_map.64 = bf16[1,160,2048]{2,1,0:T(8,128)(2,1)} custom-call(bf16[1,160,2048]{2,1,0:T(8,128)(2,1)} %bitcast.3, bf16[1,160,1024]{2,1,0:T(8,128)(2,1)} %bitcast.4, bf16[1,160,1024]{2,1,0:T(8,128)(2,1)} %bitcast.5, bf16[2048,256]{1,0:T(8,128)(2,1)} %w_ref.1, f32[64]{0:T(128)} %qg_ref.1, f32[64]{0:T(128)} %kg_ref.1), custom_call_target="tpu_custom_call" | custom-call | tf_op jit(solution)/shard_map/pallas_call | solution.py:451
  74.1 2.0 %copy.8 = bf16[1,160,2048]{2,1,0:T(8,128)(2,1)} copy(bf16[1,160,2048]{2,1,0:T(8,128)(2,1)} %shard_map.64) | data formatting | bytes 1310720

commit v6 on v5

--- a/solution.py
+++ b/solution.py
@@ -104,8 +104,8 @@
         return 2 * div(n, 2) + self.e
 
 
-def all_slots(me, body):
-    for n in range(16):
+def all_slots(me, body, first=0):
+    for n in [(first + n) % 16 for n in range(16)]:
         if n in (12, 13):
             pl.when(n != me.own)(lambda n=n: body(n))
         else:
@@ -265,7 +265,7 @@
     loop(4, make_four)
     pl.semaphore_wait(barrier, 19)
 
-    all_slots(me, lambda n: kv_copy(n).start())
+    all_slots(me, lambda n: kv_copy(n).start(), first=12)
     kvr[0, me.own] = kvs[me.own]
 
     def make_q_four(r):
@@ -333,7 +333,8 @@
     row_scale = lambda total: 1.0 / jnp.sum(total, axis=0, keepdims=True)
     s1[...] = jnp.zeros_like(s1)
 
-    def own_keys(g):
+    def own_keys(r):
+        g = lax.rem(r + 3, 4)
         loop(GROUP, lambda r: forward(GROUP * g + r))
         make_keys(0, g)
 
@@ -346,7 +347,9 @@
         s0[at, :] = s
         return jnp.maximum(m, jnp.max(by_eight(s), axis=0))
 
-    def partner_keys(g, m):
+    def partner_keys(r, m):
+        g = lax.rem(r + 3, 4)
+
         def wait(n):
             arrival(kvr.at[1, GROUP * g + n], fw_ss.at[GROUP * g + n], fw_rs.at[GROUP * g + n]).wait_recv()
 

time: 76.2 us -> 77 us (1.010)
  Pallas kernels: 74.1 us -> 74.9 us
    pallas_call x1, Pallas kernels: 74.1 us -> 74.9 us  [on_device(): pl.pallas_call(layer, out_shape=jax.ShapeDtypeStruct((1, TOK, W_ROWS), bf...]
where the time goes in v6:
time: 77 us; the launch traced here: 76.9 us
  Pallas kernels  74.9 us (97%)
  local copies, waits for them, and re-layouts  1.98 us (3%)
    pallas_call x1, Pallas kernels, on_device(): pl.pallas_call(layer, out_shape=jax.ShapeDtypeStruct((1, TOK, W_ROWS), bf...  74.9 us
    unnamed x1, local copies, waits for them, and re-layouts  1.98 us

profile of v6, /device:TPU:2, one launch (start us, length us, event | category | flops | bytes accessed | tf_op | source)
XLA Modules:
  0.0 76.9 jit_solution(14239390763507240511)
XLA Ops:
  0.0 74.9 %shard_map.64 = bf16[1,160,2048]{2,1,0:T(8,128)(2,1)} custom-call(bf16[1,160,2048]{2,1,0:T(8,128)(2,1)} %bitcast.3, bf16[1,160,1024]{2,1,0:T(8,128)(2,1)} %bitcast.4, bf16[1,160,1024]{2,1,0:T(8,128)(2,1)} %bitcast.5, bf16[2048,256]{1,0:T(8,128)(2,1)} %w_ref.1, f32[64]{0:T(128)} %qg_ref.1, f32[64]{0:T(128)} %kg_ref.1), custom_call_target="tpu_custom_call" | custom-call | tf_op jit(solution)/shard_map/pallas_call | solution.py:454
  74.9 2.0 %copy.8 = bf16[1,160,2048]{2,1,0:T(8,128)(2,1)} copy(bf16[1,160,2048]{2,1,0:T(8,128)(2,1)} %shard_map.64) | data formatting | bytes 1310720

commit v7 on v5

--- a/solution.py
+++ b/solution.py
@@ -277,6 +277,7 @@
 
     all_slots(me, lambda n: q_copy(n).start())
     qr[me.own] = qs[me.own]
+    fw_copy(me.own).start()
     own_w = pltpu.make_async_copy(w_ref, wf.at[me.dp], own_sem)
     own_w.start()
     for copy in w_own:
@@ -286,8 +287,7 @@
         @pl.when(n != me.own)
         def _():
             arrival(kvr.at[0, n], kv_ss.at[n], kv_rs.at[n]).wait_recv()
-
-        fw_copy(n).start()
+            fw_copy(n).start()
 
 
     def make_keys(half, g):

time: 76.2 us -> 76 us (level)
  no operation moved by 1% of the time
where the time goes in v7:
time: 76 us; the launch traced here: 75.7 us
  Pallas kernels  73.7 us (97%)
  local copies, waits for them, and re-layouts  1.98 us (3%)
    pallas_call x1, Pallas kernels, on_device(): pl.pallas_call(layer, out_shape=jax.ShapeDtypeStruct((1, TOK, W_ROWS), bf...  73.7 us
    unnamed x1, local copies, waits for them, and re-layouts  1.98 us

profile of v7, /device:TPU:2, one launch (start us, length us, event | category | flops | bytes accessed | tf_op | source)
XLA Modules:
  0.0 75.7 jit_solution(1172768828057959312)
XLA Ops:
  0.0 73.7 %shard_map.64 = bf16[1,160,2048]{2,1,0:T(8,128)(2,1)} custom-call(bf16[1,160,2048]{2,1,0:T(8,128)(2,1)} %bitcast.3, bf16[1,160,1024]{2,1,0:T(8,128)(2,1)} %bitcast.4, bf16[1,160,1024]{2,1,0:T(8,128)(2,1)} %bitcast.5, bf16[2048,256]{1,0:T(8,128)(2,1)} %w_ref.1, f32[64]{0:T(128)} %qg_ref.1, f32[64]{0:T(128)} %kg_ref.1), custom_call_target="tpu_custom_call" | custom-call | tf_op jit(solution)/shard_map/pallas_call | solution.py:451
  73.8 2.0 %copy.8 = bf16[1,160,2048]{2,1,0:T(8,128)(2,1)} copy(bf16[1,160,2048]{2,1,0:T(8,128)(2,1)} %shard_map.64) | data formatting | bytes 1310720
